TPU v7x, 256 devices: a 4x2x16 block of a 4x16x16 slice. The times are simulated.
256 devices in a mesh: grp: 2 (over y), fs: 32 (over z, core), tp: 4 (over x).
Axes of the slice: x: 4, y: 2, z: 16, core: 2. Of those that a mesh axis runs over, the one named last changes fastest.
The devices are a block of a 4x16x16 slice.
Arguments:
- tokens: bfloat16 [1536, 2048], P(('grp', 'tp')), parts along dimension 0, may hold values from -6 to 6
- norm_gain: float32 [2048], P('fs'), may hold values from 0.1 to 1.9
- up_trained: float32 [2048, 8192], P('fs', 'tp'), may hold values from -0.125 to 0.125
- down_trained: float32 [2048, 8192], P('fs', 'tp'), may hold values from -0.125 to 0.125
Outputs:
- up_serving: bfloat16 [4096, 8192], P('grp', 'fs'), parts along dimension 0
- down_serving: bfloat16 [4096, 8192], P('grp', 'fs'), parts along dimension 0
- prompt_output: bfloat16 [1536, 2048], P(('grp', 'tp'), 'fs'), parts along dimension 0
There are 2 independent parts, one for each index of `grp`. A program takes and returns all parts, laid end to end along the dimension named above; an argument that names none is the same for every part. Nothing has to cross between parts.
All inputs are finite; a program needn't handle non-finite values.
Results may differ from a plain program's by a relative error of at most 0.0074.
Values may be sent and summed in bfloat16 or wider, within the bound.
No kernel may reach another device: no remote copies, remote signals or barrier semaphores. Data moves between devices by JAX's collectives and lax.ppermute only.
A program may use at most 64 MiB of HBM per device.

v0:
```python
import jax
import jax.numpy as jnp
from jax import lax
from jax.sharding import PartitionSpec as P

epsilon = 1e-06
CORES = 2


def joined_along(parts, dim):
    parts = jnp.moveaxis(parts, 0, dim)
    dims = parts.shape
    return parts.reshape(*dims[:dim], dims[dim] * dims[dim + 1], *dims[dim + 2 :])


def copy_for_each(x, axis):
    devices = lax.axis_size(axis)
    return lax.all_to_all(jnp.broadcast_to(x[None], (devices, *x.shape)), axis, 0, 0, tiled=True)


def collect(x, axis, dim):
    return joined_along(copy_for_each(x, axis), dim)


def packed(x):
    rows, cols = x.shape[-2:]
    wide = cols * 2 // 3
    tail = x[..., wide:]
    tail = jnp.concatenate([tail[..., : rows // 2, :], tail[..., rows // 2 :, :]], axis=-1)
    return jnp.concatenate([x[..., :wide], tail], axis=-2)


def unpacked(x, rows):
    wide = x.shape[-1]
    tail = x[..., rows:, :]
    tail = jnp.concatenate([tail[..., : wide // 2], tail[..., wide // 2 :]], axis=-2)
    return jnp.concatenate([x[..., :rows, :], tail], axis=-1)


def sum_at_owner(x, axis):
    devices = lax.axis_size(axis)
    rows = x.shape[0] // devices
    chips = devices // CORES
    parts = packed(x.reshape(chips, CORES, rows, x.shape[1]))
    core = lax.axis_index(axis) % CORES
    away = lax.dynamic_index_in_dim(parts, 1 - core, 1, keepdims=False)
    kept = lax.dynamic_index_in_dim(parts, core, 1, keepdims=False)
    other = lax.ppermute(away, axis, [(i, i ^ 1) for i in range(devices)])
    both = (kept.astype(jnp.float32) + other.astype(jnp.float32)).astype(jnp.bfloat16)
    same_core = [[z * CORES + c for z in range(chips)] for c in range(CORES)]
    arrived = lax.all_to_all(both, axis, 0, 0, axis_index_groups=same_core, tiled=True)
    return unpacked(arrived.astype(jnp.float32).sum(axis=0), rows)


def local(tokens, norm_gain, up_trained, down_trained):
    shards = lax.axis_size("fs")
    groups = lax.axis_size("tp")
    rows_local = up_trained.shape[0]
    cols_local = up_trained.shape[1]
    folded = (norm_gain[:, None] * up_trained).astype(jnp.bfloat16)
    stacked = jnp.stack([folded, down_trained.astype(jnp.bfloat16)])
    served_width = cols_local * groups // shards
    blocks_here = cols_local // served_width
    quarter_rows = rows_local // groups
    pieces = stacked.reshape(2, groups, quarter_rows, blocks_here, served_width)
    moved = lax.all_to_all(pieces, "tp", split_axis=1, concat_axis=3, tiled=True)
    placed = lax.all_to_all(moved, "fs", split_axis=3, concat_axis=2, tiled=True)
    ordered = placed.reshape(2, shards, quarter_rows, served_width)
    joined = collect(ordered, "tp", 2)
    owned = joined.reshape(2, rows_local * shards, served_width)
    up_serving = owned[0]
    down_serving = owned[1]
    values = tokens.astype(jnp.float32)
    scale = lax.rsqrt(jnp.mean(values * values, axis=1, keepdims=True) + epsilon)
    normed = (values * scale).astype(jnp.bfloat16)
    hidden = jnp.dot(normed, up_serving, preferred_element_type=jnp.float32)
    active = jnp.square(jax.nn.relu(hidden)).astype(jnp.bfloat16)
    partial = lax.dot_general(
        down_serving, active, (((1,), (1,)), ((), ())), preferred_element_type=jnp.float32
    ).astype(jnp.bfloat16)
    prompt_output = sum_at_owner(partial, "fs").T.astype(jnp.bfloat16)
    return (up_serving, down_serving, prompt_output)


def solution(mesh):
    in_specs = (P(("grp", "tp"), None), P("fs"), P("fs", "tp"), P("fs", "tp"))
    out_specs = (P("grp", "fs"), P("grp", "fs"), P(("grp", "tp"), "fs"))
    return jax.shard_map(local, mesh=mesh, in_specs=in_specs, out_specs=out_specs, check_vma=False)
```

profile of v0, /device:TPU:40, one launch (start us, length us, event | category | flops | bytes accessed | tf_op | source)
XLA Modules:
  0.0 141.5 jit_solution(10750599824275625618)
XLA Ops:
  0.6 0.0 copy-start.3
  0.6 1.1 convert_element_type.38
  1.8 0.1 copy.24
  1.8 0.0 copy-done.3
  1.8 0.8 multiply_convert_fusion
  2.6 0.1 copy.23
  2.7 0.1 pad_maximum_fusion
  2.8 13.9 %all_to_all.43 = bf16[2,4,16,8,256]{4,3,2,0,1:T(8,128)(2,1)S(1)} all-to-all(bf16[2,4,16,8,256]{4,3,2,0,1:T(8,128)(2,1)S(1)} %copy.17), channel_id=1, replica_groups=mesh['grp'=2,'fs'=32,'tp'=4] {'tp'}, dimensions={1} | all-to-all | bytes 1048576 | tf_op jit(solution)/shard_map/all_to_all | solution.py:66
  16.7 0.1 copy.28
  16.8 0.3 copy.19
  17.1 57.6 %all_to_all.44 = bf16[2,1,16,32,256]{4,2,0,1,3:T(8,128)(2,1)S(1)} all-to-all(bf16[2,1,16,32,256]{4,2,0,1,3:T(8,128)(2,1)S(1)} %copy.19), channel_id=1, replica_groups=mesh['grp'=2,'fs'=32,'tp'=4] {'fs'}, dimensions={3} | all-to-all | bytes 1048576 | tf_op jit(solution)/shard_map/all_to_all | solution.py:67
  74.7 1.5 %broadcast_in_dim.10 = bf16[4,2,32,16,256]{4,3,2,1,0:T(8,128)(2,1)} broadcast(bf16[2,32,16,256]{3,2,1,0:T(8,128)(2,1)S(1)} %copy.20), dimensions={1,2,3,4} | broadcast | bytes 2621440 | tf_op jit(solution)/shard_map/broadcast_in_dim | solution.py:18
  76.2 0.0 copy-start.2
  76.2 3.8 %all-to-all-start.2 = ((bf16[4,2,32,16,256]{4,3,2,1,0:T(8,128)(2,1)}), bf16[4,2,32,16,256]{4,3,2,1,0:T(8,128)(2,1)S(1)}, u32[]{:S(2)}, u32[]{:S(2)}) async-start(bf16[4,2,32,16,256]{4,3,2,1,0:T(8,128)(2,1)} %broadcast_in_dim.10), calls=%async_computation.2 | async-start | bytes 4194304 | tf_op jit(solution)/shard_map/all_to_all | solution.py:18
  80.1 0.0 copy-done.2
  80.1 0.2 fusion
  80.4 26.4 %all-to-all-done.2 = bf16[4,2,32,16,256]{4,3,2,1,0:T(8,128)(2,1)S(1)} async-done(((bf16[4,2,32,16,256]{4,3,2,1,0:T(8,128)(2,1)}), bf16[4,2,32,16,256]{4,3,2,1,0:T(8,128)(2,1)S(1)}, u32[]{:S(2)}, u32[]{:S(2)}) %all-to-all-start.2) | async-done | bytes 2097184 | tf_op jit(solution)/shard_map/all_to_all | solution.py:18
  106.8 0.3 copy.27
  107.1 0.2 fusion.11
  107.3 0.0 copy-start
  107.3 0.0 copy-start.1
  107.3 2.0 %convolution_convert_fusion = bf16[2048,192]{0,1:T(8,128)(2,1)} fusion(bf16[2048,256]{1,0:T(8,128)(2,1)S(1)} %bitcast.36, bf16[2048,256]{1,0:T(8,128)(2,1)S(1)} %bitcast.38, bf16[192,2048]{1,0:T(8,128)(2,1)S(1)} %copy-done.2, f32[192]{0:T(256)S(1)} %add_rsqrt_fusion), kind=kOutput, calls=%fused_computation | convolution fusion | flops 404373504 | bytes 3670784 | tf_op jit(solution)/shard_map/dot_general | solution.py:78
  109.4 0.0 copy-done
  109.4 0.0 copy-done.1
  109.4 1.4 %copy.22 = bf16[2048,192]{1,0:T(8,128)(2,1)S(1)} copy(bf16[2048,192]{0,1:T(8,128)(2,1)} %convolution_convert_fusion) | data formatting | bytes 1572864 | tf_op jit(solution)/shard_map/convert_element_type | solution.py:80
  110.8 0.1 fusion.12
  110.9 0.1 slice.45
  111.1 0.2 maximum_maximum_fusion
  111.3 0.1 collective-permute-start
  111.5 1.7 %collective-permute-done = bf16[16,96,128]{2,1,0:T(8,128)(2,1)S(1)} collective-permute-done((bf16[16,96,128]{2,1,0:T(8,128)(2,1)S(1)}, bf16[16,96,128]{2,1,0:T(8,128)(2,1)S(1)}, u32[]{:S(2)}, u32[]{:S(2)}) %collective-permute-start) | collective-permute-done | bytes 393248 | tf_op jit(solution)/shard_map/ppermute | solution.py:48
  113.1 0.1 fusion.6
  113.3 27.5 %all_to_all.45 = bf16[16,96,128]{2,1,0:T(8,128)(2,1)S(1)} all-to-all(bf16[16,96,128]{2,1,0:T(8,128)(2,1)S(1)} %fusion.6), channel_id=1, replica_groups={{0,8,16,24,32,40,48,56,64,72,80,88,96,104,112,120},{4,12,20,28,36,44,52..., dimensions={0} | all-to-all | bytes 786432 | tf_op jit(solution)/shard_map/all_to_all | solution.py:51
  140.8 0.1 reduce
  140.8 0.1 fusion.13
  140.9 0.6 maximum_bitcast_fusion
  (5 shorter events, 0.1 us)
Async XLA Ops:
  0.6 1.2 copy-start.3
  76.2 3.9 %copy-start.2 = (bf16[192,2048]{1,0:T(8,128)(2,1)S(1)}, bf16[192,2048]{1,0:T(8,128)(2,1)}, u32[]{:S(2)}) copy-start(bf16[192,2048]{1,0:T(8,128)(2,1)} %param.4) | copy-start | bytes 2359300
  76.2 30.5 %all-to-all-start.2 = ((bf16[4,2,32,16,256]{4,3,2,1,0:T(8,128)(2,1)}), bf16[4,2,32,16,256]{4,3,2,1,0:T(8,128)(2,1)S(1)}, u32[]{:S(2)}, u32[]{:S(2)}) async-start(bf16[4,2,32,16,256]{4,3,2,1,0:T(8,128)(2,1)} %broadcast_in_dim.10), calls=%async_computation.2 | async-start | bytes 4194304 | tf_op jit(solution)/shard_map/all_to_all | solution.py:18
  107.3 2.1 %copy-start = (bf16[1,32,4,16,256]{4,3,2,1,0:T(8,128)(2,1)}, bf16[1,32,4,16,256]{4,3,2,1,0:T(8,128)(2,1)S(1)}, u32[]{:S(2)}) copy-start(bf16[1,32,4,16,256]{4,3,2,1,0:T(8,128)(2,1)S(1)} %get-tuple-element.3) | copy-start | bytes 3145732
  107.3 2.1 %copy-start.1 = (bf16[1,32,4,16,256]{4,3,2,1,0:T(8,128)(2,1)}, bf16[1,32,4,16,256]{4,3,2,1,0:T(8,128)(2,1)S(1)}, u32[]{:S(2)}) copy-start(bf16[1,32,4,16,256]{4,3,2,1,0:T(8,128)(2,1)S(1)} %get-tuple-element.4) | copy-start | bytes 3145732
  111.3 1.8 %collective-permute-start = (bf16[16,96,128]{2,1,0:T(8,128)(2,1)S(1)}, bf16[16,96,128]{2,1,0:T(8,128)(2,1)S(1)}, u32[]{:S(2)}, u32[]{:S(2)}) collective-permute-start(bf16[16,96,128]{2,1,0:T(8,128)(2,1)S(1)} %dynamic-slice_bitcast_fusion), channel_id=1, source_target_pairs={{0,4},{4,0},{8,12},{12,8},{16,20},{20,16},{24,28},{28,24},{32,36},... | collective-permute-start | bytes 1179656 | tf_op jit(solution)/shard_map/ppermute | solution.py:48
where the time goes:
time: 142 us
  blocking collectives  99.1 us (70%)
  waiting for transfers between devices  28.1 us (20%)
  local copies, waits for them, and re-layouts  4.34 us (3%)
  starting transfers between devices  3.97 us (3%)
  other arithmetic  3.16 us (2%)
  matrix products  2.05 us (1%)
    all_to_all x1, blocking collectives, local(): lax.all_to_all(moved, 'fs', split_axis=3, concat_axis=2, tiled=True)  57.6 us
    all_to_all x1, blocking collectives, sum_at_owner(): lax.all_to_all(both, axis, 0, 0, axis_index_groups=same_core, tiled=True)  27.5 us
    all_to_all x1, waiting for transfers between devices, copy_for_each(): lax.all_to_all(jnp.broadcast_to(x[None], (devices, *x.shape)), axis, 0, 0...  26.4 us
    all_to_all x1, blocking collectives, local(): lax.all_to_all(pieces, 'tp', split_axis=1, concat_axis=3, tiled=True)  13.9 us
    all_to_all x1, starting transfers between devices, copy_for_each(): lax.all_to_all(jnp.broadcast_to(x[None], (devices, *x.shape)), axis, 0, 0...  3.83 us
  transfers between devices with their start and end apart: 2, of which 2 were waited for; matrix products, arithmetic and copies ran while one was open for 0% of the time, Pallas kernels for 0%

commit v1 on v0

--- a/solution.py
+++ b/solution.py
@@ -64,7 +64,9 @@
     quarter_rows = rows_local // groups
     pieces = stacked.reshape(2, groups, quarter_rows, blocks_here, served_width)
     moved = lax.all_to_all(pieces, "tp", split_axis=1, concat_axis=3, tiled=True)
-    placed = lax.all_to_all(moved, "fs", split_axis=3, concat_axis=2, tiled=True)
+    blocks = jnp.split(moved, lax.axis_size("fs"), axis=3)
+    received = lax.all_to_all(jnp.stack(blocks), "fs", 0, 0)
+    placed = jnp.concatenate(received, axis=2)
     ordered = placed.reshape(2, shards, quarter_rows, served_width)
     joined = collect(ordered, "tp", 2)
     owned = joined.reshape(2, rows_local * shards, served_width)

time: 142 us -> 143 us (level)
  no operation moved by 1% of the time
where the time goes in v1:
time: 143 us; the launch traced here: 142 us
  blocking collectives  99.1 us (69%)
  waiting for transfers between devices  28.1 us (20%)
  local copies, waits for them, and re-layouts  5.4 us (4%)
  starting transfers between devices  3.97 us (3%)
  other arithmetic  2.51 us (2%)
  matrix products  2.05 us (1%)
    all_to_all x1, blocking collectives, local(): received = lax.all_to_all(jnp.stack(blocks), 'fs', 0, 0)  57.6 us
    all_to_all x1, blocking collectives, sum_at_owner(): lax.all_to_all(both, axis, 0, 0, axis_index_groups=same_core, tiled=True)  27.5 us
    all_to_all x1, waiting for transfers between devices, copy_for_each(): lax.all_to_all(jnp.broadcast_to(x[None], (devices, *x.shape)), axis, 0, 0...  26.4 us
    all_to_all x1, blocking collectives, local(): lax.all_to_all(pieces, 'tp', split_axis=1, concat_axis=3, tiled=True)  13.9 us
    all_to_all x1, starting transfers between devices, copy_for_each(): lax.all_to_all(jnp.broadcast_to(x[None], (devices, *x.shape)), axis, 0, 0...  3.83 us
  transfers between devices with their start and end apart: 2, of which 2 were waited for; matrix products, arithmetic and copies ran while one was open for 0% of the time, Pallas kernels for 0%

profile of v1, /device:TPU:40, one launch (start us, length us, event | category | flops | bytes accessed | tf_op | source)
XLA Modules:
  0.0 142.2 jit_solution(573584219087924942)
XLA Ops:
  0.6 0.0 copy-start.3
  0.6 1.2 multiply_convert_fusion
  1.8 0.1 copy.664
  1.9 0.0 copy-done.3
  2.0 0.1 copy.665
  2.0 0.1 pad_maximum_fusion
  2.1 13.9 %all_to_all.33 = bf16[2,4,16,8,256]{4,3,2,0,1:T(8,128)(2,1)S(1)} all-to-all(bf16[2,4,16,8,256]{4,3,2,0,1:T(8,128)(2,1)S(1)} %copy.625), channel_id=1, replica_groups=mesh['grp'=2,'fs'=32,'tp'=4] {'tp'}, dimensions={1} | all-to-all | bytes 1048576 | tf_op jit(solution)/shard_map/all_to_all | solution.py:66
  16.0 0.1 copy_bitcast_fusion
  16.1 0.5 fusion.14
  16.6 0.7 fusion.13
  17.8 57.6 %all_to_all.34 = bf16[32,2,1,16,1,256]{5,3,1,4,2,0:T(8,128)(2,1)S(1)} all-to-all(bf16[32,2,1,16,1,256]{5,3,1,4,2,0:T(8,128)(2,1)S(1)} %constant_dynamic-update-slice_fusion), channel_id=1, replica_groups=mesh['grp'=2,'fs'=32,'tp'=4] {'fs'}, dimensions={0} | all-to-all | bytes 1048576 | tf_op jit(solution)/shard_map/all_to_all | solution.py:68
  75.4 1.5 %broadcast_in_dim.10 = bf16[4,2,32,16,256]{4,3,2,1,0:T(8,128)(2,1)} broadcast(bf16[2,32,16,256]{3,2,1,0:T(8,128)(2,1)S(1)} %copy.628), dimensions={1,2,3,4} | broadcast | bytes 2621440 | tf_op jit(solution)/shard_map/broadcast_in_dim | solution.py:18
  77.0 0.0 copy-start.2
  77.0 3.8 %all-to-all-start.2 = ((bf16[4,2,32,16,256]{4,3,2,1,0:T(8,128)(2,1)}), bf16[4,2,32,16,256]{4,3,2,1,0:T(8,128)(2,1)S(1)}, u32[]{:S(2)}, u32[]{:S(2)}) async-start(bf16[4,2,32,16,256]{4,3,2,1,0:T(8,128)(2,1)} %broadcast_in_dim.10), calls=%async_computation.2 | async-start | bytes 4194304 | tf_op jit(solution)/shard_map/all_to_all | solution.py:18
  80.8 0.0 copy-done.2
  80.8 0.2 fusion
  81.1 26.4 %all-to-all-done.2 = bf16[4,2,32,16,256]{4,3,2,1,0:T(8,128)(2,1)S(1)} async-done(((bf16[4,2,32,16,256]{4,3,2,1,0:T(8,128)(2,1)}), bf16[4,2,32,16,256]{4,3,2,1,0:T(8,128)(2,1)S(1)}, u32[]{:S(2)}, u32[]{:S(2)}) %all-to-all-start.2) | async-done | bytes 2097184 | tf_op jit(solution)/shard_map/all_to_all | solution.py:18
  107.5 0.2 fusion.11
  107.7 0.1 copy.629
  107.9 0.0 copy-start
  107.9 0.1 copy.630
  108.0 0.0 copy-start.1
  108.0 2.1 %convolution_convert_fusion = bf16[2048,192]{0,1:T(8,128)(2,1)} fusion(bf16[2048,256]{1,0:T(8,128)(2,1)S(1)} %bitcast.98, bf16[2048,256]{1,0:T(8,128)(2,1)S(1)} %bitcast.96, bf16[192,2048]{1,0:T(8,128)(2,1)S(1)} %copy-done.2, f32[192]{0:T(256)S(1)} %add_rsqrt_fusion), kind=kOutput, calls=%fused_computation | convolution fusion | flops 404373504 | bytes 3670784 | tf_op jit(solution)/shard_map/dot_general | solution.py:80
  110.1 0.0 copy-done
  110.1 0.0 copy-done.1
  110.1 1.4 %copy.631 = bf16[2048,192]{1,0:T(8,128)(2,1)S(1)} copy(bf16[2048,192]{0,1:T(8,128)(2,1)} %convolution_convert_fusion) | data formatting | bytes 1572864 | tf_op jit(solution)/shard_map/convert_element_type | solution.py:82
  111.5 0.1 fusion.12
  111.6 0.1 slice.45
  111.7 0.2 maximum_maximum_fusion
  112.0 0.1 collective-permute-start
  112.1 1.7 %collective-permute-done = bf16[16,96,128]{2,1,0:T(8,128)(2,1)S(1)} collective-permute-done((bf16[16,96,128]{2,1,0:T(8,128)(2,1)S(1)}, bf16[16,96,128]{2,1,0:T(8,128)(2,1)S(1)}, u32[]{:S(2)}, u32[]{:S(2)}) %collective-permute-start) | collective-permute-done | bytes 393248 | tf_op jit(solution)/shard_map/ppermute | solution.py:48
  113.8 0.1 fusion.6
  113.9 27.5 %all_to_all.35 = bf16[16,96,128]{2,1,0:T(8,128)(2,1)S(1)} all-to-all(bf16[16,96,128]{2,1,0:T(8,128)(2,1)S(1)} %fusion.6), channel_id=1, replica_groups={{0,8,16,24,32,40,48,56,64,72,80,88,96,104,112,120},{4,12,20,28,36,44,52..., dimensions={0} | all-to-all | bytes 786432 | tf_op jit(solution)/shard_map/all_to_all | solution.py:51
  141.4 0.1 reduce
  141.5 0.1 fusion.15
  141.6 0.6 maximum_bitcast_fusion
  (38 shorter events, 0.4 us)
Async XLA Ops:
  0.6 1.3 copy-start.3
  77.0 3.9 %copy-start.2 = (bf16[192,2048]{1,0:T(8,128)(2,1)S(1)}, bf16[192,2048]{1,0:T(8,128)(2,1)}, u32[]{:S(2)}) copy-start(bf16[192,2048]{1,0:T(8,128)(2,1)} %param.4) | copy-start | bytes 2359300
  77.0 30.5 %all-to-all-start.2 = ((bf16[4,2,32,16,256]{4,3,2,1,0:T(8,128)(2,1)}), bf16[4,2,32,16,256]{4,3,2,1,0:T(8,128)(2,1)S(1)}, u32[]{:S(2)}, u32[]{:S(2)}) async-start(bf16[4,2,32,16,256]{4,3,2,1,0:T(8,128)(2,1)} %broadcast_in_dim.10), calls=%async_computation.2 | async-start | bytes 4194304 | tf_op jit(solution)/shard_map/all_to_all | solution.py:18
  107.9 2.2 %copy-start = (bf16[1,32,4,16,256]{4,3,2,1,0:T(8,128)(2,1)}, bf16[1,32,4,16,256]{4,3,2,1,0:T(8,128)(2,1)S(1)}, u32[]{:S(2)}) copy-start(bf16[1,32,4,16,256]{4,3,2,1,0:T(8,128)(2,1)S(1)} %copy.629) | copy-start | bytes 3145732
  108.0 2.1 %copy-start.1 = (bf16[1,32,4,16,256]{4,3,2,1,0:T(8,128)(2,1)}, bf16[1,32,4,16,256]{4,3,2,1,0:T(8,128)(2,1)S(1)}, u32[]{:S(2)}) copy-start(bf16[1,32,4,16,256]{4,3,2,1,0:T(8,128)(2,1)S(1)} %copy.630) | copy-start | bytes 3145732
  112.0 1.8 %collective-permute-start = (bf16[16,96,128]{2,1,0:T(8,128)(2,1)S(1)}, bf16[16,96,128]{2,1,0:T(8,128)(2,1)S(1)}, u32[]{:S(2)}, u32[]{:S(2)}) collective-permute-start(bf16[16,96,128]{2,1,0:T(8,128)(2,1)S(1)} %dynamic-slice_bitcast_fusion), channel_id=1, source_target_pairs={{0,4},{4,0},{8,12},{12,8},{16,20},{20,16},{24,28},{28,24},{32,36},... | collective-permute-start | bytes 1179656 | tf_op jit(solution)/shard_map/ppermute | solution.py:48
